TPU v7x, 32 devices: a whole 2x2x4 slice. The times are simulated.
32 devices in a mesh: fs: 8 (over z, y), tp: 4 (over x, core).
Axes of the slice: x: 2, y: 2, z: 4, core: 2. Of those that a mesh axis runs over, the one named last changes fastest.
Arguments:
- saved_inputs: bfloat16 [4096, 3072], P('fs'), may hold values from -6 to 6
- query_cotangent: bfloat16 [4096, 3072], P('fs', 'tp'), may hold values from -0.75 to 0.75
- attn_outputs: bfloat16 [4096, 3072], P('fs', 'tp'), may hold values from -6 to 6
- out_cotangent: bfloat16 [4096, 3072], P('fs'), may hold values from -0.75 to 0.75
- left_factor: bfloat16 [3072, 384], P('fs', 'tp'), may hold values from -0.109375 to 0.109375
- right_factor: bfloat16 [3072, 384], P('fs', 'tp'), may hold values from -0.109375 to 0.109375
- query_master: float32 [3072, 3072], P('fs', 'tp'), may hold values from -0.109375 to 0.109375
- out_master: float32 [3072, 3072], P('tp', 'fs'), may hold values from -0.109375 to 0.109375
- first_moment: float32 [2, 384, 3072], P(None, 'fs', 'tp'), may hold values from -14 to 14
- second_moment: float32 [2, 384, 3072], P(None, 'fs', 'tp'), may hold values from 0.3 to 3
Outputs:
- query_new: float32 [3072, 3072], P('fs', 'tp')
- out_new: float32 [3072, 3072], P('tp', 'fs')
- query_copy: bfloat16 [3072, 3072], P(None, 'tp')
- out_copy: bfloat16 [3072, 3072], P('tp')
- first_new: float32 [2, 384, 3072], P(None, 'fs', 'tp')
- second_new: float32 [2, 384, 3072], P(None, 'fs', 'tp')
All inputs are finite; a program needn't handle non-finite values.
Results may differ from a plain program's by a relative error of at most 0.0025.
Values may be sent and summed in bfloat16 or wider, within the bound.
A program may use at most 64 MiB of HBM per device.

v0:
```python
import jax
import jax.numpy as jnp
from jax import lax
from jax.sharding import PartitionSpec as P


def moment_step(first, second, grads):
    first_next = 0.9 * first + 0.1 * grads
    second_next = 0.99 * second + 0.01 * grads * grads
    return (first_next, second_next, first_next / (jnp.sqrt(second_next) + 1e-08))


def body(
    saved_inputs,
    query_cotangent,
    attn_outputs,
    out_cotangent,
    left_factor,
    right_factor,
    query_master,
    out_master,
    first_moment,
    second_moment,
):
    left_part = jnp.dot(
        saved_inputs,
        lax.all_gather(left_factor, "fs", axis=0, tiled=True),
        preferred_element_type=jnp.float32,
    )
    right_part = jnp.dot(
        out_cotangent,
        lax.all_gather(right_factor, "fs", axis=0, tiled=True),
        preferred_element_type=jnp.float32,
    )
    left_proj, right_proj, left_rows, right_rows = (
        lax.all_gather(left_part.astype(jnp.bfloat16), "tp", axis=1, tiled=True),
        lax.all_gather(right_part.astype(jnp.bfloat16), "tp", axis=1, tiled=True),
        lax.all_gather(left_factor, "tp", axis=1, tiled=True),
        lax.all_gather(right_factor, "tp", axis=1, tiled=True),
    )
    rows = first_moment.shape[1]
    dims = (((0,), (0,)), ((), ()))
    grad_query = lax.dot_general(
        left_proj, query_cotangent, dims, preferred_element_type=jnp.float32
    )
    grad_output = lax.dot_general(
        right_proj, attn_outputs, dims, preferred_element_type=jnp.float32
    )
    summed = lax.psum_scatter(
        jnp.stack([grad_query, grad_output], axis=1), "fs", scatter_dimension=0, tiled=True
    )
    grads = jnp.transpose(summed, (1, 0, 2))
    first_new, second_new, own_direction = moment_step(first_moment, second_moment, grads)
    direction_all = lax.all_gather(own_direction.astype(jnp.bfloat16), "fs", axis=1, tiled=True)
    squares = jnp.sum(own_direction * own_direction, axis=(1, 2))
    total = lax.psum(squares, ("fs", "tp"))
    entries = rows * lax.axis_size("fs") * own_direction.shape[2] * lax.axis_size("tp")
    scale = lax.rsqrt(total / entries + 1e-06)
    step_query = scale[0] * jnp.dot(left_rows, direction_all[0], preferred_element_type=jnp.float32)
    step_output = scale[1] * lax.dot_general(
        direction_all[1], right_rows, (((0,), (1,)), ((), ())), preferred_element_type=jnp.float32
    )
    query_new = query_master - 0.01 * step_query
    out_new = out_master - 0.01 * step_output
    query_copy, out_copy = (
        lax.all_gather(query_new.astype(jnp.bfloat16), "fs", axis=0, tiled=True),
        lax.all_gather(out_new.astype(jnp.bfloat16), "fs", axis=1, tiled=True),
    )
    return (query_new, out_new, query_copy, out_copy, first_new, second_new)


def solution(mesh):
    return jax.shard_map(
        body,
        mesh=mesh,
        in_specs=(
            P("fs", None),
            P("fs", "tp"),
            P("fs", "tp"),
            P("fs", None),
            P("fs", "tp"),
            P("fs", "tp"),
            P("fs", "tp"),
            P("tp", "fs"),
            P(None, "fs", "tp"),
            P(None, "fs", "tp"),
        ),
        out_specs=(
            P("fs", "tp"),
            P("tp", "fs"),
            P(None, "tp"),
            P("tp", None),
            P(None, "fs", "tp"),
            P(None, "fs", "tp"),
        ),
        check_vma=False,
    )
```

profile of v0, /device:TPU:0, one launch (start us, length us, event | category | flops | bytes accessed | tf_op | source)
XLA Modules:
  0.0 390.2 jit_solution(14397979788832499997)
XLA Ops:
  7.2 0.0 reduce-scatter.2.cloned.1.call-start
  7.2 33.9 %all_gather.27 = bf16[3072,96]{0,1:T(8,128)(2,1)S(1)} all-gather(bf16[384,96]{0,1:T(8,128)(2,1)} %param.14), channel_id=1, replica_groups=mesh['fs'=8,'tp'=4] {'fs'}, dimensions={0}, use_global_device_ids=true | all-gather | bytes 663552 | tf_op jit(solution)/shard_map/all_gather | solution.py:27
  41.1 1.1 convolution_convert_fusion.1
  42.2 6.5 %all_gather.28 = bf16[512,384]{0,1:T(8,128)(2,1)S(1)} all-gather(bf16[512,96]{0,1:T(8,128)(2,1)S(1)} %convolution_convert_fusion.1), channel_id=1, replica_groups=mesh['fs'=8,'tp'=4] {'tp'}, dimensions={1}, use_global_device_ids=true | all-gather | bytes 491520 | tf_op jit(solution)/shard_map/all_gather | solution.py:36
  48.7 31.5 %all_gather.29 = bf16[3072,96]{0,1:T(8,128)(2,1)S(1)} all-gather(bf16[384,96]{0,1:T(8,128)(2,1)S(1)} %copy-done.8), channel_id=1, replica_groups=mesh['fs'=8,'tp'=4] {'fs'}, dimensions={0}, use_global_device_ids=true | all-gather | bytes 663552 | tf_op jit(solution)/shard_map/all_gather | solution.py:32
  80.2 1.1 convolution_convert_fusion
  81.3 6.1 %all_gather.30 = bf16[512,384]{0,1:T(8,128)(2,1)S(1)} all-gather(bf16[512,96]{0,1:T(8,128)(2,1)S(1)} %convolution_convert_fusion), channel_id=1, replica_groups=mesh['fs'=8,'tp'=4] {'tp'}, dimensions={1}, use_global_device_ids=true | all-gather | bytes 491520 | tf_op jit(solution)/shard_map/all_gather | solution.py:37
  87.5 0.5 convolution_bitcast_fusion
  87.9 0.7 copy-done.5
  88.6 0.5 convolution_bitcast_fusion.1
  89.1 1.6 pad_maximum_fusion
  90.6 0.0 reduce-scatter.2.cloned.1.call-update
  90.7 0.0 all-gather.4.cloned.1.call-start
  90.7 70.5 %reduce-scatter.2.cloned.1.call-done = f32[48,2,768]{2,0,1:T(8,128)} async-done(((f32[384,2,768]{2,0,1:T(8,128)}), f32[48,2,768]{2,0,1:T(8,128)}) %reduce-scatter.2.cloned.1.call-update) | async-done | bytes 294928 | tf_op jit(solution)/shard_map/reduce_scatter | solution.py:49
  161.2 1.3 multiply_reduce_fusion
  162.6 0.7 copy-done.2
  163.3 0.1 copy-done.3
  163.4 0.8 fusion.7
  164.2 0.0 all-gather.6.cloned.1.call-start
  164.3 2.7 copy.19
  166.9 5.9 %all_gather.32 = bf16[384,384]{0,1:T(8,128)(2,1)S(1)} all-gather(bf16[384,96]{0,1:T(8,128)(2,1)S(1)} %copy-done.7), channel_id=1, replica_groups=mesh['fs'=8,'tp'=4] {'tp'}, dimensions={1}, use_global_device_ids=true | all-gather | bytes 368640 | tf_op jit(solution)/shard_map/all_gather | solution.py:38
  172.8 40.3 %psum.7 = f32[2]{0:T(128)S(1)} all-reduce(f32[2]{0:T(128)S(1)} %get-tuple-element.18), channel_id=1, replica_groups=mesh['fs'=8,'tp'=4] {'fs','tp'}, use_global_device_ids=true, to_apply=%region_2.0 | all-reduce | flops 2 | bytes 16 | tf_op jit(solution)/shard_map/psum | solution.py:56
  213.1 0.6 fusion.10
  213.7 3.8 fusion.11
  217.5 0.0 all-gather.8.cloned.1.call-start
  217.6 6.7 %all_gather.33 = bf16[384,384]{0,1:T(8,128)(2,1)S(1)} all-gather(bf16[384,96]{0,1:T(8,128)(2,1)S(1)} %copy-done.9), channel_id=1, replica_groups=mesh['fs'=8,'tp'=4] {'tp'}, dimensions={1}, use_global_device_ids=true | all-gather | bytes 368640 | tf_op jit(solution)/shard_map/all_gather | solution.py:39
  224.3 3.9 fusion.12
  228.2 2.7 copy.20
  230.9 67.2 %all-gather.6.cloned.1.call-done = bf16[3072,768]{0,1:T(8,128)(2,1)} async-done(((bf16[384,768]{0,1:T(8,128)(2,1)}), bf16[3072,768]{0,1:T(8,128)(2,1)}) %all-gather.6.cloned.1.call-update) | async-done | bytes 4718608 | tf_op jit(solution)/shard_map/all_gather | solution.py:66
  298.1 6.6 %copy.21 = bf16[3072,768]{1,0:T(8,128)(2,1)} copy(bf16[3072,768]{0,1:T(8,128)(2,1)} %all-gather.6.cloned.1.call-done) | data formatting | bytes 9437184
  304.7 74.1 %all-gather.8.cloned.1.call-done = bf16[768,3072]{1,0:T(8,128)(2,1)} async-done(((bf16[768,384]{1,0:T(8,128)(2,1)}), bf16[768,3072]{1,0:T(8,128)(2,1)}) %all-gather.8.cloned.1.call-update) | async-done | bytes 4718608 | tf_op jit(solution)/shard_map/all_gather | solution.py:67
  378.8 4.8 %copy.23 = bf16[768,3072]{1,0:T(8,128)(2,1)} copy(bf16[768,3072]{1,0:T(8,128)(2,1)} %all-gather.8.cloned.1.call-done) | data formatting | bytes 9437184
  (22 shorter events, 0.1 us)
Async XLA Ops:
  7.2 33.9 %copy-start = (bf16[512,3072]{1,0:T(8,128)(2,1)S(1)}, bf16[512,3072]{1,0:T(8,128)(2,1)}, u32[]{:S(2)}) copy-start(bf16[512,3072]{1,0:T(8,128)(2,1)} %param.10) | copy-start | bytes 9437188
  7.2 154.1 %reduce-scatter.2.cloned.1.call-start = ((), (), s32[]{:S(2)}) async-start(), calls=%async_computation.1 | async-start | bytes 2654208 | tf_op jit(solution)/shard_map/reduce_scatter | solution.py:49
  41.1 7.6 %copy-start.8 = (bf16[384,96]{0,1:T(8,128)(2,1)S(1)}, bf16[384,96]{0,1:T(8,128)(2,1)}, u32[]{:S(2)}) copy-start(bf16[384,96]{0,1:T(8,128)(2,1)} %param.15) | copy-start | bytes 221188
  41.1 39.1 %copy-start.1 = (bf16[512,3072]{1,0:T(8,128)(2,1)S(1)}, bf16[512,3072]{1,0:T(8,128)(2,1)}, u32[]{:S(2)}) copy-start(bf16[512,3072]{1,0:T(8,128)(2,1)} %param.13) | copy-start | bytes 9437188
  80.2 7.3 %copy-start.4 = (bf16[512,768]{1,0:T(8,128)(2,1)S(1)}, bf16[512,768]{1,0:T(8,128)(2,1)}, u32[]{:S(2)}) copy-start(bf16[512,768]{1,0:T(8,128)(2,1)} %param.12) | copy-start | bytes 2359300
  87.5 1.1 copy-start.5
  90.6 70.6 %copy-start.6 = (f32[2,48,768]{2,1,0:T(8,128)S(1)}, f32[2,48,768]{2,1,0:T(8,128)}, u32[]{:S(2)}) copy-start(f32[2,48,768]{2,1,0:T(8,128)} %param.19) | copy-start | bytes 884740
  90.7 123.0 %all-gather.4.cloned.1.call-start = ((), (), s32[]{:S(2)}) async-start(), calls=%async_computation.2 | async-start | bytes 1327104 | tf_op jit(solution)/shard_map/all_gather | solution.py:54
  162.6 0.7 copy-start.2
  162.6 0.8 copy-start.3
  164.2 2.7 copy-start.7
  164.2 133.9 %all-gather.6.cloned.1.call-start = ((), (), s32[]{:S(2)}) async-start(), calls=%async_computation.3 | async-start | bytes 5308416 | tf_op jit(solution)/shard_map/all_gather | solution.py:66
  213.7 3.9 %copy-start.9 = (bf16[384,96]{0,1:T(8,128)(2,1)S(1)}, bf16[384,96]{0,1:T(8,128)(2,1)}, u32[]{:S(2)}) copy-start(bf16[384,96]{0,1:T(8,128)(2,1)} %param.15) | copy-start | bytes 221188
  217.5 161.2 %all-gather.8.cloned.1.call-start = ((), (), s32[]{:S(2)}) async-start(), calls=%async_computation.4 | async-start | bytes 5308416 | tf_op jit(solution)/shard_map/all_gather | solution.py:67
Sparse Core Ops, SparseCore 0:
  90.8 70.4 reduce-scatter.1
  164.3 40.5 all-gather.3
  217.7 80.3 all-gather.5
  300.0 78.7 all-gather.7
where the time goes:
time: 391 us; the launch traced here: 390 us
  waiting for transfers between devices  212 us (54%)
  blocking collectives  131 us (34%)
  local copies, waits for them, and re-layouts  18.8 us (5%)
  between operations  13.8 us (4%)
  matrix products  10.9 us (3%)
    all_gather x1, waiting for transfers between devices, body(): lax.all_gather(out_new.astype(jnp.bfloat16), 'fs', axis=1, tiled=True)  74.1 us
    reduce_scatter x1, waiting for transfers between devices, body(): lax.psum_scatter(jnp.stack([grad_query, grad_output], axis=1), 'fs', scat...  70.5 us
    all_gather x1, waiting for transfers between devices, body(): lax.all_gather(query_new.astype(jnp.bfloat16), 'fs', axis=0, tiled=True)  67.2 us
    psum x1, blocking collectives, body(): total = lax.psum(squares, ('fs', 'tp'))  40.3 us
    all_gather x1, blocking collectives, body(): lax.all_gather(left_factor, 'fs', axis=0, tiled=True)  33.9 us
    all_gather x1, blocking collectives, body(): lax.all_gather(right_factor, 'fs', axis=0, tiled=True)  31.5 us
    unnamed x24, local copies, waits for them, and re-layouts  18.3 us
  transfers between devices with their start and end apart: 4, of which 3 were waited for; matrix products, arithmetic and copies ran while one was open for 4% of the time, Pallas kernels for 0%

commit v1 on v0

--- a/solution.py
+++ b/solution.py
@@ -53,7 +53,8 @@
     first_new, second_new, own_direction = moment_step(first_moment, second_moment, grads)
     direction_all = lax.all_gather(own_direction.astype(jnp.bfloat16), "fs", axis=1, tiled=True)
     squares = jnp.sum(own_direction * own_direction, axis=(1, 2))
-    total = lax.psum(squares, ("fs", "tp"))
+    one_axis = lax.psum(squares, "tp")
+    total = lax.psum(one_axis, "fs")
     entries = rows * lax.axis_size("fs") * own_direction.shape[2] * lax.axis_size("tp")
     scale = lax.rsqrt(total / entries + 1e-06)
     step_query = scale[0] * jnp.dot(left_rows, direction_all[0], preferred_element_type=jnp.float32)

time: 391 us -> 381 us (0.974)
  blocking collectives: 131 us -> 116 us
  waiting for transfers between devices: 212 us -> 216 us
    psum x1 -> x2, blocking collectives: 40.3 us -> 26.5 us  [the longest x1 19.1 us: body(): total = lax.psum(one_axis, 'fs')]
    all_gather x1, waiting for transfers between devices: 0.01 us -> 4.88 us  [body(): lax.all_gather(own_direction.astype(jnp.bfloat16), 'fs', axis=1, tiled=True)]
  transfers between devices with their start and end apart: 4 -> 4, of which waited for: 3 -> 4; matrix products, arithmetic and copies ran while one was open for 4% -> 4% of each run, Pallas kernels for 0% -> 0%
where the time goes in v1:
time: 381 us; the launch traced here: 380 us
  waiting for transfers between devices  216 us (57%)
  blocking collectives  116 us (30%)
  local copies, waits for them, and re-layouts  18.9 us (5%)
  between operations  13.8 us (4%)
  matrix products  10.9 us (3%)
    all_gather x1, waiting for transfers between devices, body(): lax.all_gather(out_new.astype(jnp.bfloat16), 'fs', axis=1, tiled=True)  74.1 us
    reduce_scatter x1, waiting for transfers between devices, body(): lax.psum_scatter(jnp.stack([grad_query, grad_output], axis=1), 'fs', scat...  70.5 us
    all_gather x1, waiting for transfers between devices, body(): lax.all_gather(query_new.astype(jnp.bfloat16), 'fs', axis=0, tiled=True)  66.9 us
    all_gather x1, blocking collectives, body(): lax.all_gather(left_factor, 'fs', axis=0, tiled=True)  33.9 us
    all_gather x1, blocking collectives, body(): lax.all_gather(right_factor, 'fs', axis=0, tiled=True)  31.5 us
    psum x1, blocking collectives, body(): total = lax.psum(one_axis, 'fs')  19.1 us
    unnamed x24, local copies, waits for them, and re-layouts  18.3 us
  transfers between devices with their start and end apart: 4, of which 4 were waited for; matrix products, arithmetic and copies ran while one was open for 4% of the time, Pallas kernels for 0%

profile of v1, /device:TPU:0, one launch (start us, length us, event | category | flops | bytes accessed | tf_op | source)
XLA Modules:
  0.0 380.3 jit_solution(9525001210661544813)
XLA Ops:
  7.2 33.9 %all_gather.27 = bf16[3072,96]{0,1:T(8,128)(2,1)S(1)} all-gather(bf16[384,96]{0,1:T(8,128)(2,1)} %param.14), channel_id=1, replica_groups=mesh['fs'=8,'tp'=4] {'fs'}, dimensions={0}, use_global_device_ids=true | all-gather | bytes 663552 | tf_op jit(solution)/shard_map/all_gather | solution.py:27
  41.1 1.1 convolution_convert_fusion.1
  42.2 6.5 %all_gather.28 = bf16[512,384]{0,1:T(8,128)(2,1)S(1)} all-gather(bf16[512,96]{0,1:T(8,128)(2,1)S(1)} %convolution_convert_fusion.1), channel_id=1, replica_groups=mesh['fs'=8,'tp'=4] {'tp'}, dimensions={1}, use_global_device_ids=true | all-gather | bytes 491520 | tf_op jit(solution)/shard_map/all_gather | solution.py:36
  48.7 31.5 %all_gather.29 = bf16[3072,96]{0,1:T(8,128)(2,1)S(1)} all-gather(bf16[384,96]{0,1:T(8,128)(2,1)S(1)} %copy-done.8), channel_id=1, replica_groups=mesh['fs'=8,'tp'=4] {'fs'}, dimensions={0}, use_global_device_ids=true | all-gather | bytes 663552 | tf_op jit(solution)/shard_map/all_gather | solution.py:32
  80.2 1.1 convolution_convert_fusion
  81.3 6.1 %all_gather.30 = bf16[512,384]{0,1:T(8,128)(2,1)S(1)} all-gather(bf16[512,96]{0,1:T(8,128)(2,1)S(1)} %convolution_convert_fusion), channel_id=1, replica_groups=mesh['fs'=8,'tp'=4] {'tp'}, dimensions={1}, use_global_device_ids=true | all-gather | bytes 491520 | tf_op jit(solution)/shard_map/all_gather | solution.py:37
  87.5 0.5 convolution_bitcast_fusion
  87.9 0.7 copy-done.5
  88.6 0.5 convolution_bitcast_fusion.1
  89.1 1.6 pad_maximum_fusion
  90.7 0.0 all-gather.4.cloned.1.call-start
  90.7 70.5 %reduce-scatter.2.cloned.1.call-done = f32[48,2,768]{2,0,1:T(8,128)} async-done(((f32[384,2,768]{2,0,1:T(8,128)}), f32[48,2,768]{2,0,1:T(8,128)}) %reduce-scatter.2.cloned.1.call-update) | async-done | bytes 294928 | tf_op jit(solution)/shard_map/reduce_scatter | solution.py:49
  161.2 1.3 multiply_reduce_fusion
  162.6 0.7 copy-done.2
  163.3 0.1 copy-done.3
  163.4 0.8 fusion.7
  164.2 0.0 all-gather.6.cloned.1.call-start
  164.2 5.9 %all_gather.32 = bf16[384,384]{0,1:T(8,128)(2,1)S(1)} all-gather(bf16[384,96]{0,1:T(8,128)(2,1)S(1)} %copy-done.7), channel_id=1, replica_groups=mesh['fs'=8,'tp'=4] {'tp'}, dimensions={1}, use_global_device_ids=true | all-gather | bytes 368640 | tf_op jit(solution)/shard_map/all_gather | solution.py:38
  170.2 7.4 %psum.14 = f32[2]{0:T(128)S(1)} all-reduce(f32[2]{0:T(128)S(1)} %get-tuple-element.18), channel_id=1, replica_groups=mesh['fs'=8,'tp'=4] {'tp'}, use_global_device_ids=true, to_apply=%region_2.0 | all-reduce | flops 2 | bytes 16 | tf_op jit(solution)/shard_map/psum | solution.py:56
  177.6 2.7 copy.19
  180.2 19.1 %psum.15 = f32[2]{0:T(128)S(1)} all-reduce(f32[2]{0:T(128)S(1)} %psum.14), channel_id=1, replica_groups=mesh['fs'=8,'tp'=4] {'fs'}, use_global_device_ids=true, to_apply=%region_3.0 | all-reduce | flops 2 | bytes 16 | tf_op jit(solution)/shard_map/psum | solution.py:57
  199.3 0.6 fusion.10
  199.9 4.9 %all-gather.4.cloned.1.call-done = bf16[2,384,768]{2,1,0:T(8,128)(2,1)} async-done(((bf16[2,48,768]{2,1,0:T(8,128)(2,1)}), bf16[2,384,768]{2,1,0:T(8,128)(2,1)}) %all-gather.4.cloned.1.call-update) | async-done | bytes 1179664 | tf_op jit(solution)/shard_map/all_gather | solution.py:54
  204.8 3.9 %fusion.11 = (bf16[384,768]{0,1:T(8,128)(2,1)}, f32[384,768]{0,1:T(8,128)}) fusion(f32[384,768]{0,1:T(8,128)} %copy.19, bf16[384,384]{0,1:T(8,128)(2,1)S(1)} %all_gather.32, bf16[2,384,768]{2,1,0:T(8,128)(2,1)} %all-gather.4.cloned.1.call-done, f32[]{:T(128)} %bitcast.3), kind=kOutput, calls=%fused_computation.23 | convolution fusion | flops 227672064 | bytes 3834368 | tf_op jit(solution)/shard_map/dot_general | solution.py:60
  208.8 0.0 all-gather.8.cloned.1.call-start
  208.8 5.9 %all_gather.33 = bf16[384,384]{0,1:T(8,128)(2,1)S(1)} all-gather(bf16[384,96]{0,1:T(8,128)(2,1)S(1)} %copy-done.9), channel_id=1, replica_groups=mesh['fs'=8,'tp'=4] {'tp'}, dimensions={1}, use_global_device_ids=true | all-gather | bytes 368640 | tf_op jit(solution)/shard_map/all_gather | solution.py:39
  214.7 3.9 %fusion.12 = (bf16[768,384]{1,0:T(8,128)(2,1)}, f32[768,384]{1,0:T(8,128)}) fusion(f32[768,384]{1,0:T(8,128)} %param.17, bf16[384,384]{0,1:T(8,128)(2,1)S(1)} %all_gather.33, bf16[2,384,768]{2,1,0:T(8,128)(2,1)} %all-gather.4.cloned.1.call-done, f32[]{:T(128)} %bitcast.6), kind=kOutput, calls=%fused_computation.24 | convolution fusion | flops 227672064 | bytes 3834368 | tf_op jit(solution)/shard_map/dot_general | solution.py:61
  218.6 2.7 copy.20
  221.3 66.9 %all-gather.6.cloned.1.call-done = bf16[3072,768]{0,1:T(8,128)(2,1)} async-done(((bf16[384,768]{0,1:T(8,128)(2,1)}), bf16[3072,768]{0,1:T(8,128)(2,1)}) %all-gather.6.cloned.1.call-update) | async-done | bytes 4718608 | tf_op jit(solution)/shard_map/all_gather | solution.py:67
  288.2 6.6 %copy.21 = bf16[3072,768]{1,0:T(8,128)(2,1)} copy(bf16[3072,768]{0,1:T(8,128)(2,1)} %all-gather.6.cloned.1.call-done) | data formatting | bytes 9437184
  294.8 74.1 %all-gather.8.cloned.1.call-done = bf16[768,3072]{1,0:T(8,128)(2,1)} async-done(((bf16[768,384]{1,0:T(8,128)(2,1)}), bf16[768,3072]{1,0:T(8,128)(2,1)}) %all-gather.8.cloned.1.call-update) | async-done | bytes 4718608 | tf_op jit(solution)/shard_map/all_gather | solution.py:68
  368.9 4.8 %copy.23 = bf16[768,3072]{1,0:T(8,128)(2,1)} copy(bf16[768,3072]{1,0:T(8,128)(2,1)} %all-gather.8.cloned.1.call-done) | data formatting | bytes 9437184
  (23 shorter events, 0.2 us)
Async XLA Ops:
  7.2 33.9 %copy-start = (bf16[512,3072]{1,0:T(8,128)(2,1)S(1)}, bf16[512,3072]{1,0:T(8,128)(2,1)}, u32[]{:S(2)}) copy-start(bf16[512,3072]{1,0:T(8,128)(2,1)} %param.10) | copy-start | bytes 9437188
  7.2 154.1 %reduce-scatter.2.cloned.1.call-start = ((), (), s32[]{:S(2)}) async-start(), calls=%async_computation.1 | async-start | bytes 2654208 | tf_op jit(solution)/shard_map/reduce_scatter | solution.py:49
  41.1 7.6 %copy-start.8 = (bf16[384,96]{0,1:T(8,128)(2,1)S(1)}, bf16[384,96]{0,1:T(8,128)(2,1)}, u32[]{:S(2)}) copy-start(bf16[384,96]{0,1:T(8,128)(2,1)} %param.15) | copy-start | bytes 221188
  41.1 39.1 %copy-start.1 = (bf16[512,3072]{1,0:T(8,128)(2,1)S(1)}, bf16[512,3072]{1,0:T(8,128)(2,1)}, u32[]{:S(2)}) copy-start(bf16[512,3072]{1,0:T(8,128)(2,1)} %param.13) | copy-start | bytes 9437188
  80.2 7.3 %copy-start.4 = (bf16[512,768]{1,0:T(8,128)(2,1)S(1)}, bf16[512,768]{1,0:T(8,128)(2,1)}, u32[]{:S(2)}) copy-start(bf16[512,768]{1,0:T(8,128)(2,1)} %param.12) | copy-start | bytes 2359300
  87.5 1.1 copy-start.5
  90.6 70.6 %copy-start.6 = (f32[2,48,768]{2,1,0:T(8,128)S(1)}, f32[2,48,768]{2,1,0:T(8,128)}, u32[]{:S(2)}) copy-start(f32[2,48,768]{2,1,0:T(8,128)} %param.19) | copy-start | bytes 884740
  90.7 73.6 %copy-start.7 = (bf16[384,96]{0,1:T(8,128)(2,1)S(1)}, bf16[384,96]{0,1:T(8,128)(2,1)}, u32[]{:S(2)}) copy-start(bf16[384,96]{0,1:T(8,128)(2,1)} %param.14) | copy-start | bytes 221188
  90.7 114.1 %all-gather.4.cloned.1.call-start = ((), (), s32[]{:S(2)}) async-start(), calls=%async_computation.2 | async-start | bytes 1327104 | tf_op jit(solution)/shard_map/all_gather | solution.py:54
  162.6 0.7 copy-start.2
  162.6 0.8 copy-start.3
  164.2 124.0 %all-gather.6.cloned.1.call-start = ((), (), s32[]{:S(2)}) async-start(), calls=%async_computation.3 | async-start | bytes 5308416 | tf_op jit(solution)/shard_map/all_gather | solution.py:67
  204.8 4.0 %copy-start.9 = (bf16[384,96]{0,1:T(8,128)(2,1)S(1)}, bf16[384,96]{0,1:T(8,128)(2,1)}, u32[]{:S(2)}) copy-start(bf16[384,96]{0,1:T(8,128)(2,1)} %param.15) | copy-start | bytes 221188
  208.8 160.1 %all-gather.8.cloned.1.call-start = ((), (), s32[]{:S(2)}) async-start(), calls=%async_computation.4 | async-start | bytes 5308416 | tf_op jit(solution)/shard_map/all_gather | solution.py:68
Sparse Core Ops, SparseCore 0:
  90.8 70.4 reduce-scatter.1
  164.3 40.4 all-gather.3
  208.9 79.2 all-gather.5
  290.1 78.7 all-gather.7
